TPU v7x, 32 devices: a whole 2x2x4 slice. The times are simulated.
32 devices in a mesh: grp: 2 (over y), tp: 4 (over z), dp: 4 (over x, core).
Axes of the slice: x: 2, y: 2, z: 4, core: 2. Of those that a mesh axis runs over, the one named last changes fastest.
Arguments:
- tokens: bfloat16 [128, 4096], P('grp', 'dp'), parts along dimension 0, may hold values from -6 to 6
- norm_gain: float32 [2, 4096], P(None, 'dp'), may hold values from 0.1 to 1.9
- w_query: bfloat16 [2, 4096, 512], P(None, 'dp', 'tp'), may hold values from -0.09375 to 0.09375
- w_key: bfloat16 [2, 4096, 512], P(None, 'dp', 'tp'), may hold values from -0.09375 to 0.09375
- w_value: bfloat16 [2, 4096, 512], P(None, 'dp', 'tp'), may hold values from -0.09375 to 0.09375
- w_outgate: bfloat16 [2, 4096, 512], P(None, 'dp', 'tp'), may hold values from -0.09375 to 0.09375
- gate_weight: bfloat16 [2, 4, 384, 2], P(None, 'tp'), may hold values from -0.3125 to 0.3125
- forget_bias: float32 [2, 4], P(None, 'tp'), may hold values from -2 to 4
- w_mix: bfloat16 [2, 512, 4096], P(None, 'tp', 'dp'), may hold values from -0.25 to 0.25
- memory: float32 [2, 128, 4, 128, 128], P(None, ('grp', 'dp'), 'tp'), parts along dimension 1, may hold values from -3 to 3
- normalizer: float32 [2, 128, 4, 128], P(None, ('grp', 'dp'), 'tp'), parts along dimension 1, may hold values from -3 to 3
- stabilizer: float32 [2, 128, 4], P(None, ('grp', 'dp'), 'tp'), parts along dimension 1, may hold values from -4 to 4
Outputs:
- result: bfloat16 [128, 4096], P('grp', 'dp'), parts along dimension 0
- new_memory: float32 [2, 128, 4, 128, 128], P(None, ('grp', 'dp'), 'tp'), parts along dimension 1
- new_normalizer: float32 [2, 128, 4, 128], P(None, ('grp', 'dp'), 'tp'), parts along dimension 1
- new_stabilizer: float32 [2, 128, 4], P(None, ('grp', 'dp'), 'tp'), parts along dimension 1
There are 2 independent parts, one for each index of `grp`. A program takes and returns all parts, laid end to end along the dimension named above; an argument that names none is the same for every part. Nothing has to cross between parts.
All inputs are finite; a program needn't handle non-finite values.
Results may differ from a plain program's by a relative error of at most 0.018.
Values may be sent and summed in bfloat16 or wider, within the bound.
No kernel may reach another device: no remote copies, remote signals or barrier semaphores. Data moves between devices by JAX's collectives and lax.ppermute only.
A program may use at most 64 MiB of HBM per device.

v0:
```python
import functools

import jax
import jax.numpy as jnp
from jax import lax
from jax.experimental import pallas as pl
from jax.experimental.pallas import tpu as pltpu
from jax.sharding import PartitionSpec as P


EPS = 1e-06
LANES = 128


def is_pow2(n):
    return n & (n - 1) == 0


def dest(i, s, n):
    return i ^ s if is_pow2(n) else (i + s) % n


def origin(i, s, n):
    return i ^ s if is_pow2(n) else (i - s + n) % n


def shift(x, axis, s, n):
    return lax.ppermute(x, axis, [(i, dest(i, s, n)) for i in range(n)])


def fetches(w_refs, blk, stage, sems):
    return [
        pltpu.make_async_copy(w_ref.at[blk], stage.at[at], sems.at[at])
        for at, w_ref in enumerate(w_refs)]


def project(xf, gain, loads, stage, part_refs, buf, n_dp, seq_own):
    scaled_in = (xf * gain).astype(jnp.bfloat16)
    width = stage.shape[-1]
    for at, load in enumerate(loads):
        load.wait()
        buf[:, at * width:(at + 1) * width] = jnp.dot(
            scaled_in, stage[at], preferred_element_type=jnp.float32)
    squares = jnp.sum(xf * xf, axis=-1, keepdims=True)
    buf[:, len(loads) * width:] = jnp.broadcast_to(squares, (xf.shape[0], LANES))
    me = lax.axis_index("dp")
    for s in range(n_dp):
        row = pl.multiple_of(dest(me, s, n_dp) * seq_own, seq_own)
        part_refs[s][...] = buf[pl.ds(row, seq_own), :]


def columns(half, width):
    return pl.ds(pl.multiple_of(half * width, LANES), width)


def first_body(x_ref, gain_ref, wq, wk, wv, wo, mix_ref, *rest, n_dp, n_grp, seq_own):
    part_refs, mix_outs, (buf, stage, x_buf, gain_buf, sems) = rest[:n_dp], rest[n_dp:-5], rest[-5:]
    loads = fetches((wq, wk, wv, wo), 0, stage, sems)
    early = [
        pltpu.make_async_copy(x_ref, x_buf, sems.at[len(loads) + len(mix_outs)]),
        pltpu.make_async_copy(gain_ref, gain_buf, sems.at[len(loads) + len(mix_outs) + 1])]
    half = mix_ref.shape[-1] // n_grp
    cols = columns(lax.axis_index("grp"), half)
    cuts = [
        pltpu.make_async_copy(mix_ref.at[blk, :, cols], out, sems.at[len(loads) + blk])
        for blk, out in enumerate(mix_outs)]
    for copy in early + loads + cuts:
        copy.start()
    for copy in early:
        copy.wait()
    xf = x_buf[...].astype(jnp.float32)
    project(xf, gain_buf[0:1, :], loads, stage, part_refs, buf, n_dp, seq_own)
    for copy in cuts:
        copy.wait()


def mix_rows(x_buf, g_ref, early, own, others, acc, n_dp, n_tp, n_grp):
    me, grp = lax.axis_index("tp"), lax.axis_index("grp")
    half = own.shape[-1] // n_grp
    rows = [
        jnp.concatenate([g_ref[d, origin(me, s, n_tp)] for d in range(n_dp)], axis=0)
        for s in range(n_tp)]
    for copy in early:
        copy.wait()
    acc[...] = x_buf[...].astype(jnp.float32) + jnp.dot(
        rows[0], own[...], preferred_element_type=jnp.float32)
    for h in range(n_grp):
        cols = columns(origin(grp, h, n_grp), half)
        acc[:, cols] += sum(
            jnp.dot(rows[s], others[(s - 1) * n_grp + h][...], preferred_element_type=jnp.float32)
            for s in range(1, n_tp))
    return acc[...].astype(jnp.bfloat16)


def mid_body(x_ref, g_ref, mix_ref, *rest, blk, n_dp, n_tp, n_grp, seq_own):
    count = (n_tp - 1) * n_grp
    others, rest = rest[:count], rest[count:]
    gain_ref, wq, wk, wv, wo, x_out = rest[:6]
    part_refs, (acc, own, buf, stage, x_buf, gain_buf, sems) = rest[6:6 + n_dp], rest[6 + n_dp:]
    loads = fetches((wq, wk, wv, wo), blk, stage, sems)
    early = [
        pltpu.make_async_copy(mix_ref.at[blk - 1], own, sems.at[len(loads)]),
        pltpu.make_async_copy(x_ref, x_buf, sems.at[len(loads) + 1]),
        pltpu.make_async_copy(gain_ref, gain_buf, sems.at[len(loads) + 2])]
    for copy in early + loads:
        copy.start()
    x = mix_rows(x_buf, g_ref, early, own, others, acc, n_dp, n_tp, n_grp)
    x_out[...] = x
    project(x.astype(jnp.float32), gain_buf[blk:blk + 1, :], loads, stage, part_refs, buf,
            n_dp, seq_own)


def last_body(x_ref, g_ref, mix_ref, *rest, blk, n_dp, n_tp, n_grp):
    others, (x_out, acc, own, x_buf, sems) = rest[:-5], rest[-5:]
    early = [
        pltpu.make_async_copy(mix_ref.at[blk], own, sems.at[0]),
        pltpu.make_async_copy(x_ref, x_buf, sems.at[1])]
    for copy in early:
        copy.start()
    x_out[...] = mix_rows(x_buf, g_ref, early, own, others, acc, n_dp, n_tp, n_grp)


def cell_body(bias, *refs, blk, n_dp, width, copies):
    parts, refs = refs[:n_dp], refs[n_dp:]
    gw_ref, mem_far, norm_ref, stab_ref, send_ref, keep_out, added_out, value_out, stab_out = refs[:9]
    mem_ref, sems = refs[9:]
    chunks = sems.shape[0]
    span = mem_ref.shape[0] // chunks
    loads = [
        pltpu.make_async_copy(
            mem_far.at[blk, pl.ds(c * span, span), 0], mem_ref.at[pl.ds(c * span, span)], sems.at[c])
        for c in range(chunks)]
    for copy in loads:
        copy.start()
    total = parts[0][...]
    for part in parts[1:]:
        total = total + part[...]
    dk = mem_ref.shape[-1]
    scale = lax.rsqrt(total[:, 4 * dk:4 * dk + 1] / width + EPS)
    q16, k16, v16, o16 = ((scale * total[:, a * dk:(a + 1) * dk]).astype(jnp.bfloat16) for a in range(4))
    query, key, value, outgate = (t.astype(jnp.float32) for t in (q16, k16, v16, o16))
    pre = sum(
        lax.dot_general(t, gw_ref[blk, 0, :, a * dk:(a + 1) * dk], (((1,), (1,)), ((), ())),
                        preferred_element_type=jnp.float32)
        for a, t in enumerate((q16, k16, v16)))
    log_input = pre[:, 0:1]
    z = pre[:, 1:2] + bias[0, blk]
    log_forget = jnp.minimum(z, 0.0) - jnp.log1p(jnp.exp(-jnp.abs(z)))
    stab = jnp.broadcast_to(stab_ref[blk], (LANES, stab_ref.shape[-1])).T
    carried = log_forget + stab[:, 0:1]
    new_stab = jnp.maximum(carried, log_input)
    keep = jnp.exp(carried - new_stab)
    admit = jnp.exp(log_input - new_stab)
    added = admit * (key * dk ** (-0.5))
    new_norm = keep * norm_ref[blk, :, 0, :] + added
    denom = jnp.maximum(jnp.abs(jnp.sum(query * new_norm, axis=-1, keepdims=True)), 1.0)
    query_t = query.T
    numer = []
    for s in range(query.shape[0]):
        if s % span == 0:
            loads[s // span].wait()
        numer.append(jnp.sum(query_t[:, s:s + 1] * mem_ref[s], axis=0, keepdims=True))
    overlap = jnp.sum(query * added, axis=-1, keepdims=True)
    readout = (keep * jnp.concatenate(numer, axis=0) + overlap * value) / denom
    gated = (readout * jax.nn.sigmoid(outgate)).astype(jnp.bfloat16)
    for at in range(copies):
        send_ref[at] = gated
    keep_out[...] = jnp.broadcast_to(keep, keep_out.shape)
    added_out[...] = added
    value_out[...] = value
    stab_out[...] = jnp.broadcast_to(new_stab, stab_out.shape)


def write_body(mem_ref, norm_ref, *refs, blocks, span):
    given, (mem_out, norm_out, stab_out) = refs[:4 * blocks], refs[4 * blocks:]
    for blk in range(blocks):
        @pl.when(pl.program_id(0) == blk)
        def _(blk=blk):
            keep_ref, added_ref, value_ref, stab_ref = given[4 * blk:4 * blk + 4]
            rows = pl.ds(pl.multiple_of(pl.program_id(1) * span, span), span)
            keep, added, value = keep_ref[rows, :], added_ref[rows, :], value_ref[rows, :]
            added_t = added.T
            for s in range(span):
                mem_out[0, s, 0] = (
                    keep[s:s + 1, :] * mem_ref[0, s, 0] + added_t[:, s:s + 1] * value[s:s + 1, :])
            norm_out[0, :, 0, :] = keep * norm_ref[0, :, 0, :] + added
            stab_out[0] = stab_ref[...].T[0:1, :]


VMEM = pl.BlockSpec(memory_space=pltpu.VMEM)
SMEM = pl.BlockSpec(memory_space=pltpu.SMEM)
ANY = pl.BlockSpec(memory_space=pl.ANY)


NEAR_BYTES = 2 ** 21


def near(x, room):
    return pltpu.with_memory_space_constraint(x, pltpu.VMEM) if room else x


class Far:
    def __init__(self, array):
        self.array = array


def kernel_call(body, ins, outs, scratch=(), far=False, scalars=()):
    room = sum(t.nbytes for t in ins if not isinstance(t, Far)) <= 2 * NEAR_BYTES
    out = pl.pallas_call(
        body,
        out_shape=[
            o.array if isinstance(o, Far) else o if isinstance(o, jax.ShapeDtypeStruct) else jax.ShapeDtypeStruct(*o) if far else pltpu.VMEM(*o)
            for o in outs],
        in_specs=[SMEM] * len(scalars) + [ANY if isinstance(t, Far) else VMEM for t in ins],
        out_specs=[ANY if isinstance(o, Far) else VMEM for o in outs],
        scratch_shapes=list(scratch),
    )(*scalars, *(t.array if isinstance(t, Far) else near(t, room or t.nbytes < NEAR_BYTES // 32) for t in ins))
    return list(out)


def shards(tokens, norm_gain, w_query, w_key, w_value, w_outgate, gate_weight, forget_bias, w_mix,
           memory, normalizer, stabilizer, *, n_dp, n_tp, n_grp):
    blocks, seq_own, heads_own, dk, _ = memory.shape
    assert heads_own == 1
    weights = [Far(w) for w in (w_query, w_key, w_value, w_outgate)]
    far_mix = Far(w_mix)
    rows, feats = tokens.shape
    wide = 4 * w_query.shape[-1] + LANES
    part_shapes = [((seq_own, wide), jnp.float32)] * n_dp
    buf = pltpu.VMEM((rows, wide), jnp.float32)
    acc = pltpu.VMEM((rows, feats), jnp.float32)
    stage = pltpu.VMEM((len(weights),) + w_query.shape[1:], w_query.dtype)
    own_mix = pltpu.VMEM(w_mix.shape[1:], w_mix.dtype)
    sems = pltpu.SemaphoreType.DMA((len(weights) + blocks + 2,))
    x_shape = (tokens.shape, tokens.dtype)
    sizes = dict(n_dp=n_dp, n_tp=n_tp, n_grp=n_grp)
    x_buf = pltpu.VMEM(*x_shape)
    gain_buf = pltpu.VMEM(norm_gain.shape, norm_gain.dtype)
    far_gain = Far(norm_gain)
    gate_t = gate_weight.swapaxes(2, 3)
    stab_t = stabilizer.swapaxes(1, 2)
    bias_t = forget_bias.T

    out = kernel_call(
        functools.partial(first_body, n_dp=n_dp, n_grp=n_grp, seq_own=seq_own),
        [Far(tokens), far_gain, *weights, far_mix],
        part_shapes + [Far(jax.ShapeDtypeStruct((w_mix.shape[1], feats // n_grp), w_mix.dtype))] * blocks,
        [buf, stage, x_buf, gain_buf, sems])
    parts, own_mixes = out[:n_dp], out[n_dp:]

    x = tokens
    given = []
    gathered = None
    for blk in range(blocks):
        if gathered is not None:
            out = kernel_call(
                functools.partial(mid_body, blk=blk, seq_own=seq_own, **sizes),
                [Far(x), gathered, far_mix, *mixes, far_gain, *weights],
                [jax.ShapeDtypeStruct(*x_shape)] + part_shapes, [acc, own_mix, buf, stage, x_buf, gain_buf, sems])
            x, parts = out[0], out[1:]
        arrived = [parts[0]] + [shift(parts[s], "dp", s, n_dp) for s in range(1, n_dp)]
        own = own_mixes[blk]
        if gathered is not None:
            own, _ = lax.optimization_barrier((own, x))
        pieces = [shift(own, "tp", s, n_tp) for s in range(1, n_tp)]
        small = ((seq_own, dk), jnp.float32)
        out = kernel_call(
            functools.partial(cell_body, blk=blk, n_dp=n_dp, width=feats * n_dp, copies=n_dp * n_tp),
            [*arrived, gate_t, Far(memory), normalizer, stab_t],
            [((n_dp * n_tp, seq_own, dk), jnp.bfloat16)] + [small] * 4,
            [pltpu.VMEM((seq_own, dk, dk), memory.dtype), pltpu.SemaphoreType.DMA((4,))],
            scalars=(bias_t,))
        given += out[1:]
        gathered = lax.all_to_all(out[0], ("dp", "tp"), 0, 0, tiled=True)
        gathered = gathered.reshape(n_dp, n_tp, seq_own, dk)
        mixes = []
        for piece in pieces:
            piece, _ = lax.optimization_barrier((piece, out[1]))
            mixes += [piece] + [shift(piece, "grp", h, n_grp) for h in range(1, n_grp)]
    span = seq_own // 2
    state_specs = [
        pl.BlockSpec((1, span, 1, dk, dk), lambda b, c: (b, c, 0, 0, 0)),
        pl.BlockSpec((1, span, 1, dk), lambda b, c: (b, c, 0, 0))]
    new_mem, new_norm, new_stab = pl.pallas_call(
        functools.partial(write_body, blocks=blocks, span=span),
        out_shape=[jax.ShapeDtypeStruct(t.shape, t.dtype) for t in (memory, normalizer, stab_t)],
        grid=(blocks, seq_own // span),
        in_specs=state_specs + [VMEM] * len(given),
        out_specs=state_specs + [pl.BlockSpec((1, 1, seq_own), lambda b, c: (b, 0, 0))],
        name="write_state",
    )(memory, normalizer, *(near(t, True) for t in given))
    (x,) = kernel_call(
        functools.partial(last_body, blk=blocks - 1, **sizes),
        [Far(x), gathered, far_mix, *mixes], [x_shape], [acc, own_mix, x_buf, sems],
        far=True)
    return x, new_mem, new_norm, new_stab.swapaxes(1, 2)


def solution(mesh):
    in_specs = (
        P("grp", "dp"),
        P(None, "dp"),
        P(None, "dp", "tp"),
        P(None, "dp", "tp"),
        P(None, "dp", "tp"),
        P(None, "dp", "tp"),
        P(None, "tp", None, None),
        P(None, "tp"),
        P(None, "tp", "dp"),
        P(None, ("grp", "dp"), "tp", None, None),
        P(None, ("grp", "dp"), "tp", None),
        P(None, ("grp", "dp"), "tp"),
    )
    out_specs = (
        P("grp", "dp"),
        P(None, ("grp", "dp"), "tp", None, None),
        P(None, ("grp", "dp"), "tp", None),
        P(None, ("grp", "dp"), "tp"),
    )
    body = functools.partial(shards, n_dp=mesh.shape["dp"], n_tp=mesh.shape["tp"],
                             n_grp=mesh.shape["grp"])
    return jax.shard_map(body, mesh=mesh, in_specs=in_specs, out_specs=out_specs, check_vma=False)
```

profile of v0, /device:TPU:0, one launch (start us, length us, event | category | flops | bytes accessed | tf_op | source)
XLA Modules:
  0.0 70.1 jit_solution(10098740431556060684)
XLA Ops:
  0.6 0.0 copy-start
  0.7 9.1 %shard_map.147 = (f32[16,640]{1,0:T(8,128)S(1)}, f32[16,640]{1,0:T(8,128)S(1)}, f32[16,640]{1,0:T(8,128)S(1)}, f32[16,640]{1,0:T(8,128)S(1)}, bf16[128,512]{1,0:T(8,128)(2,1)}, /*index=5*/bf16[128,512]{1,0:T(8,128)(2,1)}) custom-call(bf16[64,1024]{1,0:T(8,128)(2,1)} %x_ref.3, f32[2,1024]{1,0:T(2,128)} %rest_6_.1, bf16[2,1024,128]{2,1,0:T(8,128)(2,1)} %rest_7_.1, ...), custom_call_target="tpu_custom_call" | custom-call | tf_op jit(solution)/shard_map/pallas_call | solution.py:209
  9.8 5.1 %collective-permute-start.7 = (bf16[128,512]{1,0:T(8,128)(2,1)}, bf16[128,512]{1,0:T(8,128)(2,1)S(1)}, u32[]{:S(2)}, u32[]{:S(2)}) collective-permute-start(bf16[128,512]{1,0:T(8,128)(2,1)} %get-tuple-element.40), channel_id=1, source_target_pairs={{0,12},{4,8},{8,4},{12,0},{1,13},{5,9},{9,5},{13,1},{2,14},{6,10},... | collective-permute-start | bytes 393224 | tf_op jit(solution)/shard_map/ppermute | solution.py:28
  14.9 0.0 collective-permute-start.5
  15.0 0.6 collective-permute-start.3
  15.6 0.0 collective-permute-start
  15.6 1.6 %collective-permute-start.1 = (f32[16,640]{1,0:T(8,128)S(1)}, f32[16,640]{1,0:T(8,128)S(1)}, u32[]{:S(2)}, u32[]{:S(2)}) collective-permute-start(f32[16,640]{1,0:T(8,128)S(1)} %get-tuple-element.37), channel_id=1, source_target_pairs={{0,2},{1,3},{2,0},{3,1},{4,6},{5,7},{6,4},{7,5},{8,10},{9,11},{10,... | collective-permute-start | bytes 122888 | tf_op jit(solution)/shard_map/ppermute | solution.py:28
  17.2 0.0 collective-permute-done.refs_1_
  17.2 1.0 %collective-permute-start.2 = (f32[16,640]{1,0:T(8,128)S(1)}, f32[16,640]{1,0:T(8,128)S(1)}, u32[]{:S(2)}, u32[]{:S(2)}) collective-permute-start(f32[16,640]{1,0:T(8,128)S(1)} %get-tuple-element.38), channel_id=1, source_target_pairs={{0,3},{1,2},{2,1},{3,0},{4,7},{5,6},{6,5},{7,4},{8,11},{9,10},{10,... | collective-permute-start | bytes 122888 | tf_op jit(solution)/shard_map/ppermute | solution.py:28
  18.2 1.4 %collective-permute-done.1.refs_2_ = f32[16,640]{1,0:T(8,128)S(1)} collective-permute-done((f32[16,640]{1,0:T(8,128)S(1)}, f32[16,640]{1,0:T(8,128)S(1)}, u32[]{:S(2)}, u32[]{:S(2)}) %collective-permute-start.1) | collective-permute-done | bytes 40992 | tf_op jit(solution)/shard_map/ppermute | solution.py:28
  19.6 1.1 %collective-permute-done.2.refs_3_ = f32[16,640]{1,0:T(8,128)S(1)} collective-permute-done((f32[16,640]{1,0:T(8,128)S(1)}, f32[16,640]{1,0:T(8,128)S(1)}, u32[]{:S(2)}, u32[]{:S(2)}) %collective-permute-start.2) | collective-permute-done | bytes 40992 | tf_op jit(solution)/shard_map/ppermute | solution.py:28
  20.7 0.0 copy-done
  20.7 2.6 %shard_map.148 = (bf16[16,16,128]{2,1,0:T(8,128)(2,1)S(1)}, f32[16,128]{1,0:T(8,128)S(1)}, f32[16,128]{1,0:T(8,128)S(1)}, f32[16,128]{1,0:T(8,128)S(1)}, f32[16,128]{1,0:T(8,128)S(1)}) custom-call(f32[1,2]{1,0:T(1,128)} %bitcast.16, f32[16,640]{1,0:T(8,128)S(1)} %get-tuple-element.35.refs_0_, f32[16,640]{1,0:T(8,128)S(1)} %collective-permute-done.refs_1_, ...), custom_call_target="tpu_custom_call" | custom-call | tf_op jit(solution)/shard_map/pallas_call | solution.py:209
  23.3 0.0 copy-start.3
  23.3 0.0 collective-permute-done.7.rest_4_
  23.3 1.6 %collective-permute-start.8 = (bf16[128,512]{1,0:T(8,128)(2,1)S(1)}, bf16[128,512]{1,0:T(8,128)(2,1)S(1)}, u32[]{:S(2)}, u32[]{:S(2)}) collective-permute-start(bf16[128,512]{1,0:T(8,128)(2,1)S(1)} %collective-permute-done.7.rest_4_), channel_id=1, source_target_pairs={{0,16},{16,0},{1,17},{17,1},{2,18},{18,2},{3,19},{19,3},{4,20},{20... | collective-permute-start | bytes 393224 | tf_op jit(solution)/shard_map/ppermute | solution.py:28
  24.9 1.3 %collective-permute-done.5.rest_2_ = bf16[128,512]{1,0:T(8,128)(2,1)S(1)} collective-permute-done((bf16[128,512]{1,0:T(8,128)(2,1)}, bf16[128,512]{1,0:T(8,128)(2,1)S(1)}, u32[]{:S(2)}, u32[]{:S(2)}) %collective-permute-start.5) | collective-permute-done | bytes 131104 | tf_op jit(solution)/shard_map/ppermute | solution.py:28
  26.2 1.5 %collective-permute-start.6 = (bf16[128,512]{1,0:T(8,128)(2,1)S(1)}, bf16[128,512]{1,0:T(8,128)(2,1)S(1)}, u32[]{:S(2)}, u32[]{:S(2)}) collective-permute-start(bf16[128,512]{1,0:T(8,128)(2,1)S(1)} %collective-permute-done.5.rest_2_), channel_id=1, source_target_pairs={{0,16},{16,0},{1,17},{17,1},{2,18},{18,2},{3,19},{19,3},{4,20},{20... | collective-permute-start | bytes 393224 | tf_op jit(solution)/shard_map/ppermute | solution.py:28
  27.8 0.0 collective-permute-done.3.rest_0_
  27.8 0.5 collective-permute-start.4
  28.3 11.2 %all_to_all.10 = bf16[16,16,128]{2,1,0:T(8,128)(2,1)S(1)} all-to-all(bf16[16,16,128]{2,1,0:T(8,128)(2,1)S(1)} %get-tuple-element.39), channel_id=1, replica_groups=mesh['grp'=2,'tp'=4,'dp'=4] {'dp','tp'}, dimensions={0} | all-to-all | bytes 131072 | tf_op jit(solution)/shard_map/all_to_all | solution.py:274
  39.5 0.0 collective-permute-done.8.rest_5_
  39.5 0.0 collective-permute-done.6.rest_3_
  39.5 0.0 collective-permute-done.4.rest_1_
  39.5 2.6 %shard_map.149 = (bf16[64,1024]{1,0:T(8,128)(2,1)}, f32[16,640]{1,0:T(8,128)S(1)}, f32[16,640]{1,0:T(8,128)S(1)}, f32[16,640]{1,0:T(8,128)S(1)}, f32[16,640]{1,0:T(8,128)S(1)}) custom-call(bf16[64,1024]{1,0:T(8,128)(2,1)} %x_ref.3, bf16[4,4,16,128]{3,2,1,0:T(8,128)(2,1)S(1)} %bitcast.10, bf16[2,128,1024]{2,1,0:T(8,128)(2,1)} %mix_ref.5, ...), custom_call_target="tpu_custom_call" | custom-call | tf_op jit(solution)/shard_map/pallas_call | solution.py:209
  42.1 0.8 %collective-permute-start.16 = (bf16[128,512]{1,0:T(8,128)(2,1)S(1)}, bf16[128,512]{1,0:T(8,128)(2,1)S(1)}, u32[]{:S(2)}, u32[]{:S(2)}) collective-permute-start(bf16[128,512]{1,0:T(8,128)(2,1)S(1)} %copy-done.3), channel_id=1, source_target_pairs={{0,12},{4,8},{8,4},{12,0},{1,13},{5,9},{9,5},{13,1},{2,14},{6,10},... | collective-permute-start | bytes 393224 | tf_op jit(solution)/shard_map/ppermute | solution.py:28
  42.9 1.1 %collective-permute-start.14 = (bf16[128,512]{1,0:T(8,128)(2,1)S(1)}, bf16[128,512]{1,0:T(8,128)(2,1)S(1)}, u32[]{:S(2)}, u32[]{:S(2)}) collective-permute-start(bf16[128,512]{1,0:T(8,128)(2,1)S(1)} %copy-done.3), channel_id=1, source_target_pairs={{0,8},{4,12},{8,0},{12,4},{1,9},{5,13},{9,1},{13,5},{2,10},{6,14},... | collective-permute-start | bytes 393224 | tf_op jit(solution)/shard_map/ppermute | solution.py:28
  44.0 2.6 %collective-permute-start.12 = (bf16[128,512]{1,0:T(8,128)(2,1)S(1)}, bf16[128,512]{1,0:T(8,128)(2,1)S(1)}, u32[]{:S(2)}, u32[]{:S(2)}) collective-permute-start(bf16[128,512]{1,0:T(8,128)(2,1)S(1)} %copy-done.3), channel_id=1, source_target_pairs={{0,4},{4,0},{8,12},{12,8},{1,5},{5,1},{9,13},{13,9},{2,6},{6,2},{1... | collective-permute-start | bytes 393224 | tf_op jit(solution)/shard_map/ppermute | solution.py:28
  46.6 0.0 collective-permute-start.9
  46.6 0.7 %collective-permute-start.10 = (f32[16,640]{1,0:T(8,128)S(1)}, f32[16,640]{1,0:T(8,128)S(1)}, u32[]{:S(2)}, u32[]{:S(2)}) collective-permute-start(f32[16,640]{1,0:T(8,128)S(1)} %get-tuple-element.48), channel_id=1, source_target_pairs={{0,2},{1,3},{2,0},{3,1},{4,6},{5,7},{6,4},{7,5},{8,10},{9,11},{10,... | collective-permute-start | bytes 122888 | tf_op jit(solution)/shard_map/ppermute | solution.py:28
  47.3 0.5 collective-permute-done.9.refs_1_
  47.8 0.6 collective-permute-start.11
  48.4 2.1 %collective-permute-done.10.refs_2_ = f32[16,640]{1,0:T(8,128)S(1)} collective-permute-done((f32[16,640]{1,0:T(8,128)S(1)}, f32[16,640]{1,0:T(8,128)S(1)}, u32[]{:S(2)}, u32[]{:S(2)}) %collective-permute-start.10) | collective-permute-done | bytes 40992 | tf_op jit(solution)/shard_map/ppermute | solution.py:28
  50.6 0.7 %collective-permute-done.11.refs_3_ = f32[16,640]{1,0:T(8,128)S(1)} collective-permute-done((f32[16,640]{1,0:T(8,128)S(1)}, f32[16,640]{1,0:T(8,128)S(1)}, u32[]{:S(2)}, u32[]{:S(2)}) %collective-permute-start.11) | collective-permute-done | bytes 40992 | tf_op jit(solution)/shard_map/ppermute | solution.py:28
  51.3 2.9 %shard_map.150 = (bf16[16,16,128]{2,1,0:T(8,128)(2,1)}, f32[16,128]{1,0:T(8,128)S(1)}, f32[16,128]{1,0:T(8,128)S(1)}, f32[16,128]{1,0:T(8,128)S(1)}, f32[16,128]{1,0:T(8,128)S(1)}) custom-call(f32[1,2]{1,0:T(1,128)} %bitcast.17, f32[16,640]{1,0:T(8,128)S(1)} %get-tuple-element.46.refs_0_, f32[16,640]{1,0:T(8,128)S(1)} %collective-permute-done.9.refs_1_, ...), custom_call_target="tpu_custom_call" | custom-call | tf_op jit(solution)/shard_map/pallas_call | solution.py:209
  54.2 0.0 collective-permute-done.16.rest_4_
  54.2 1.6 %collective-permute-start.17 = (bf16[128,512]{1,0:T(8,128)(2,1)S(1)}, bf16[128,512]{1,0:T(8,128)(2,1)S(1)}, u32[]{:S(2)}, u32[]{:S(2)}) collective-permute-start(bf16[128,512]{1,0:T(8,128)(2,1)S(1)} %collective-permute-done.16.rest_4_), channel_id=1, source_target_pairs={{0,16},{16,0},{1,17},{17,1},{2,18},{18,2},{3,19},{19,3},{4,20},{20... | collective-permute-start | bytes 393224 | tf_op jit(solution)/shard_map/ppermute | solution.py:28
  55.8 0.1 collective-permute-done.14.rest_2_
  55.9 1.5 %collective-permute-start.15 = (bf16[128,512]{1,0:T(8,128)(2,1)S(1)}, bf16[128,512]{1,0:T(8,128)(2,1)S(1)}, u32[]{:S(2)}, u32[]{:S(2)}) collective-permute-start(bf16[128,512]{1,0:T(8,128)(2,1)S(1)} %collective-permute-done.14.rest_2_), channel_id=1, source_target_pairs={{0,16},{16,0},{1,17},{17,1},{2,18},{18,2},{3,19},{19,3},{4,20},{20... | collective-permute-start | bytes 393224 | tf_op jit(solution)/shard_map/ppermute | solution.py:28
  57.5 0.0 collective-permute-done.12.rest_0_
  57.5 0.5 collective-permute-start.13
  58.0 3.5 %all-to-all-start.1 = ((bf16[16,16,128]{2,1,0:T(8,128)(2,1)}), bf16[16,16,128]{2,1,0:T(8,128)(2,1)S(1)}, u32[]{:S(2)}, u32[]{:S(2)}) async-start(bf16[16,16,128]{2,1,0:T(8,128)(2,1)} %get-tuple-element.50), calls=%async_computation.1 | async-start | bytes 131072 | tf_op jit(solution)/shard_map/all_to_all | solution.py:274
  61.5 4.5 %write_state.1 = (f32[2,16,1,128,128]{4,3,2,1,0:T(8,128)}, f32[2,16,1,128]{3,2,1,0:T(1,128)}, f32[2,1,16]{2,1,0:T(1,128)}) custom-call(f32[2,16,1,128,128]{4,3,2,1,0:T(8,128)} %mem_ref.1, f32[2,16,1,128]{3,2,1,0:T(1,128)} %norm_ref.1, f32[16,128]{1,0:T(8,128)S(1)} %get-tuple-element.41.refs_0_, f32[16,128]{1,0:T(8,128)S(1)} %get-tuple-element.57.refs_1_, ...), custom_call_target="tpu_custom_call" | custom-call | tf_op jit(solution)/shard_map/write_state/pallas_call | solution.py:284
  65.9 2.1 %all-to-all-done.1 = bf16[16,16,128]{2,1,0:T(8,128)(2,1)S(1)} async-done(((bf16[16,16,128]{2,1,0:T(8,128)(2,1)}), bf16[16,16,128]{2,1,0:T(8,128)(2,1)S(1)}, u32[]{:S(2)}, u32[]{:S(2)}) %all-to-all-start.1) | async-done | bytes 65568 | tf_op jit(solution)/shard_map/all_to_all | solution.py:274
  68.0 0.0 collective-permute-done.17.rest_5_
  68.0 0.0 collective-permute-done.15.rest_3_
  68.1 0.0 collective-permute-done.13.rest_1_
  68.1 2.0 %shard_map.151 = bf16[64,1024]{1,0:T(8,128)(2,1)} custom-call(bf16[64,1024]{1,0:T(8,128)(2,1)} %get-tuple-element.45.x_ref, bf16[4,4,16,128]{3,2,1,0:T(8,128)(2,1)S(1)} %bitcast.11, bf16[2,128,1024]{2,1,0:T(8,128)(2,1)} %mix_ref.5, bf16[128,512]{1,0:T(8,128)(2,1)S(1)} %collective-permute-done.12.rest_0_, ...), custom_call_target="tpu_custom_call" | custom-call | tf_op jit(solution)/shard_map/pallas_call | solution.py:209
  (5 shorter events, 0.0 us)
Async XLA Ops:
  0.6 20.1 %copy-start = (f32[2,16,1,128]{3,2,1,0:T(1,128)S(1)}, f32[2,16,1,128]{3,2,1,0:T(1,128)}, u32[]{:S(2)}) copy-start(f32[2,16,1,128]{3,2,1,0:T(1,128)} %norm_ref.1) | copy-start | bytes 49156
  0.6 20.1 %copy-start.2 = (f32[2,16,1]{1,2,0:T(1,128)S(1)}, f32[2,16,1]{1,2,0:T(1,128)}, u32[]{:S(2)}) copy-start(f32[2,16,1]{1,2,0:T(1,128)} %param.23) | copy-start | bytes 388
  0.7 20.0 %copy-start.1 = (bf16[2,1,384,2]{2,3,1,0:T(2,128)(2,1)S(1)}, bf16[2,1,384,2]{2,3,1,0:T(2,128)(2,1)}, u32[]{:S(2)}) copy-start(bf16[2,1,384,2]{2,3,1,0:T(2,128)(2,1)} %param.18) | copy-start | bytes 9220
  9.8 13.5 %collective-permute-start.7 = (bf16[128,512]{1,0:T(8,128)(2,1)}, bf16[128,512]{1,0:T(8,128)(2,1)S(1)}, u32[]{:S(2)}, u32[]{:S(2)}) collective-permute-start(bf16[128,512]{1,0:T(8,128)(2,1)} %get-tuple-element.40), channel_id=1, source_target_pairs={{0,12},{4,8},{8,4},{12,0},{1,13},{5,9},{9,5},{13,1},{2,14},{6,10},... | collective-permute-start | bytes 393224 | tf_op jit(solution)/shard_map/ppermute | solution.py:28
  14.9 11.3 %collective-permute-start.5 = (bf16[128,512]{1,0:T(8,128)(2,1)}, bf16[128,512]{1,0:T(8,128)(2,1)S(1)}, u32[]{:S(2)}, u32[]{:S(2)}) collective-permute-start(bf16[128,512]{1,0:T(8,128)(2,1)} %get-tuple-element.40), channel_id=1, source_target_pairs={{0,8},{4,12},{8,0},{12,4},{1,9},{5,13},{9,1},{13,5},{2,10},{6,14},... | collective-permute-start | bytes 393224 | tf_op jit(solution)/shard_map/ppermute | solution.py:28
  15.0 12.8 %collective-permute-start.3 = (bf16[128,512]{1,0:T(8,128)(2,1)}, bf16[128,512]{1,0:T(8,128)(2,1)S(1)}, u32[]{:S(2)}, u32[]{:S(2)}) collective-permute-start(bf16[128,512]{1,0:T(8,128)(2,1)} %get-tuple-element.40), channel_id=1, source_target_pairs={{0,4},{4,0},{8,12},{12,8},{1,5},{5,1},{9,13},{13,9},{2,6},{6,2},{1... | collective-permute-start | bytes 393224 | tf_op jit(solution)/shard_map/ppermute | solution.py:28
  15.6 1.6 %collective-permute-start = (f32[16,640]{1,0:T(8,128)S(1)}, f32[16,640]{1,0:T(8,128)S(1)}, u32[]{:S(2)}, u32[]{:S(2)}) collective-permute-start(f32[16,640]{1,0:T(8,128)S(1)} %get-tuple-element.36), channel_id=1, source_target_pairs={{0,1},{1,0},{2,3},{3,2},{4,5},{5,4},{6,7},{7,6},{8,9},{9,8},{10,11... | collective-permute-start | bytes 122888 | tf_op jit(solution)/shard_map/ppermute | solution.py:28
  15.6 4.0 %collective-permute-start.1 = (f32[16,640]{1,0:T(8,128)S(1)}, f32[16,640]{1,0:T(8,128)S(1)}, u32[]{:S(2)}, u32[]{:S(2)}) collective-permute-start(f32[16,640]{1,0:T(8,128)S(1)} %get-tuple-element.37), channel_id=1, source_target_pairs={{0,2},{1,3},{2,0},{3,1},{4,6},{5,7},{6,4},{7,5},{8,10},{9,11},{10,... | collective-permute-start | bytes 122888 | tf_op jit(solution)/shard_map/ppermute | solution.py:28
  17.2 3.5 %collective-permute-start.2 = (f32[16,640]{1,0:T(8,128)S(1)}, f32[16,640]{1,0:T(8,128)S(1)}, u32[]{:S(2)}, u32[]{:S(2)}) collective-permute-start(f32[16,640]{1,0:T(8,128)S(1)} %get-tuple-element.38), channel_id=1, source_target_pairs={{0,3},{1,2},{2,1},{3,0},{4,7},{5,6},{6,5},{7,4},{8,11},{9,10},{10,... | collective-permute-start | bytes 122888 | tf_op jit(solution)/shard_map/ppermute | solution.py:28
  23.3 18.8 %copy-start.3 = (bf16[128,512]{1,0:T(8,128)(2,1)S(1)}, bf16[128,512]{1,0:T(8,128)(2,1)}, u32[]{:S(2)}) copy-start(bf16[128,512]{1,0:T(8,128)(2,1)} %get-tuple-element.52) | copy-start | bytes 393220
  23.3 16.1 %collective-permute-start.8 = (bf16[128,512]{1,0:T(8,128)(2,1)S(1)}, bf16[128,512]{1,0:T(8,128)(2,1)S(1)}, u32[]{:S(2)}, u32[]{:S(2)}) collective-permute-start(bf16[128,512]{1,0:T(8,128)(2,1)S(1)} %collective-permute-done.7.rest_4_), channel_id=1, source_target_pairs={{0,16},{16,0},{1,17},{17,1},{2,18},{18,2},{3,19},{19,3},{4,20},{20... | collective-permute-start | bytes 393224 | tf_op jit(solution)/shard_map/ppermute | solution.py:28
  26.2 13.2 %collective-permute-start.6 = (bf16[128,512]{1,0:T(8,128)(2,1)S(1)}, bf16[128,512]{1,0:T(8,128)(2,1)S(1)}, u32[]{:S(2)}, u32[]{:S(2)}) collective-permute-start(bf16[128,512]{1,0:T(8,128)(2,1)S(1)} %collective-permute-done.5.rest_2_), channel_id=1, source_target_pairs={{0,16},{16,0},{1,17},{17,1},{2,18},{18,2},{3,19},{19,3},{4,20},{20... | collective-permute-start | bytes 393224 | tf_op jit(solution)/shard_map/ppermute | solution.py:28
  27.8 11.7 %collective-permute-start.4 = (bf16[128,512]{1,0:T(8,128)(2,1)S(1)}, bf16[128,512]{1,0:T(8,128)(2,1)S(1)}, u32[]{:S(2)}, u32[]{:S(2)}) collective-permute-start(bf16[128,512]{1,0:T(8,128)(2,1)S(1)} %collective-permute-done.3.rest_0_), channel_id=1, source_target_pairs={{0,16},{16,0},{1,17},{17,1},{2,18},{18,2},{3,19},{19,3},{4,20},{20... | collective-permute-start | bytes 393224 | tf_op jit(solution)/shard_map/ppermute | solution.py:28
  42.1 12.1 %collective-permute-start.16 = (bf16[128,512]{1,0:T(8,128)(2,1)S(1)}, bf16[128,512]{1,0:T(8,128)(2,1)S(1)}, u32[]{:S(2)}, u32[]{:S(2)}) collective-permute-start(bf16[128,512]{1,0:T(8,128)(2,1)S(1)} %copy-done.3), channel_id=1, source_target_pairs={{0,12},{4,8},{8,4},{12,0},{1,13},{5,9},{9,5},{13,1},{2,14},{6,10},... | collective-permute-start | bytes 393224 | tf_op jit(solution)/shard_map/ppermute | solution.py:28
  42.9 13.0 %collective-permute-start.14 = (bf16[128,512]{1,0:T(8,128)(2,1)S(1)}, bf16[128,512]{1,0:T(8,128)(2,1)S(1)}, u32[]{:S(2)}, u32[]{:S(2)}) collective-permute-start(bf16[128,512]{1,0:T(8,128)(2,1)S(1)} %copy-done.3), channel_id=1, source_target_pairs={{0,8},{4,12},{8,0},{12,4},{1,9},{5,13},{9,1},{13,5},{2,10},{6,14},... | collective-permute-start | bytes 393224 | tf_op jit(solution)/shard_map/ppermute | solution.py:28
  44.0 13.5 %collective-permute-start.12 = (bf16[128,512]{1,0:T(8,128)(2,1)S(1)}, bf16[128,512]{1,0:T(8,128)(2,1)S(1)}, u32[]{:S(2)}, u32[]{:S(2)}) collective-permute-start(bf16[128,512]{1,0:T(8,128)(2,1)S(1)} %copy-done.3), channel_id=1, source_target_pairs={{0,4},{4,0},{8,12},{12,8},{1,5},{5,1},{9,13},{13,9},{2,6},{6,2},{1... | collective-permute-start | bytes 393224 | tf_op jit(solution)/shard_map/ppermute | solution.py:28
  46.6 1.2 %collective-permute-start.9 = (f32[16,640]{1,0:T(8,128)S(1)}, f32[16,640]{1,0:T(8,128)S(1)}, u32[]{:S(2)}, u32[]{:S(2)}) collective-permute-start(f32[16,640]{1,0:T(8,128)S(1)} %get-tuple-element.47), channel_id=1, source_target_pairs={{0,1},{1,0},{2,3},{3,2},{4,5},{5,4},{6,7},{7,6},{8,9},{9,8},{10,11... | collective-permute-start | bytes 122888 | tf_op jit(solution)/shard_map/ppermute | solution.py:28
  46.6 4.0 %collective-permute-start.10 = (f32[16,640]{1,0:T(8,128)S(1)}, f32[16,640]{1,0:T(8,128)S(1)}, u32[]{:S(2)}, u32[]{:S(2)}) collective-permute-start(f32[16,640]{1,0:T(8,128)S(1)} %get-tuple-element.48), channel_id=1, source_target_pairs={{0,2},{1,3},{2,0},{3,1},{4,6},{5,7},{6,4},{7,5},{8,10},{9,11},{10,... | collective-permute-start | bytes 122888 | tf_op jit(solution)/shard_map/ppermute | solution.py:28
  47.8 3.5 %collective-permute-start.11 = (f32[16,640]{1,0:T(8,128)S(1)}, f32[16,640]{1,0:T(8,128)S(1)}, u32[]{:S(2)}, u32[]{:S(2)}) collective-permute-start(f32[16,640]{1,0:T(8,128)S(1)} %get-tuple-element.49), channel_id=1, source_target_pairs={{0,3},{1,2},{2,1},{3,0},{4,7},{5,6},{6,5},{7,4},{8,11},{9,10},{10,... | collective-permute-start | bytes 122888 | tf_op jit(solution)/shard_map/ppermute | solution.py:28
  54.2 13.8 %collective-permute-start.17 = (bf16[128,512]{1,0:T(8,128)(2,1)S(1)}, bf16[128,512]{1,0:T(8,128)(2,1)S(1)}, u32[]{:S(2)}, u32[]{:S(2)}) collective-permute-start(bf16[128,512]{1,0:T(8,128)(2,1)S(1)} %collective-permute-done.16.rest_4_), channel_id=1, source_target_pairs={{0,16},{16,0},{1,17},{17,1},{2,18},{18,2},{3,19},{19,3},{4,20},{20... | collective-permute-start | bytes 393224 | tf_op jit(solution)/shard_map/ppermute | solution.py:28
  55.9 12.1 %collective-permute-start.15 = (bf16[128,512]{1,0:T(8,128)(2,1)S(1)}, bf16[128,512]{1,0:T(8,128)(2,1)S(1)}, u32[]{:S(2)}, u32[]{:S(2)}) collective-permute-start(bf16[128,512]{1,0:T(8,128)(2,1)S(1)} %collective-permute-done.14.rest_2_), channel_id=1, source_target_pairs={{0,16},{16,0},{1,17},{17,1},{2,18},{18,2},{3,19},{19,3},{4,20},{20... | collective-permute-start | bytes 393224 | tf_op jit(solution)/shard_map/ppermute | solution.py:28
  57.5 10.6 %collective-permute-start.13 = (bf16[128,512]{1,0:T(8,128)(2,1)S(1)}, bf16[128,512]{1,0:T(8,128)(2,1)S(1)}, u32[]{:S(2)}, u32[]{:S(2)}) collective-permute-start(bf16[128,512]{1,0:T(8,128)(2,1)S(1)} %collective-permute-done.12.rest_0_), channel_id=1, source_target_pairs={{0,16},{16,0},{1,17},{17,1},{2,18},{18,2},{3,19},{19,3},{4,20},{20... | collective-permute-start | bytes 393224 | tf_op jit(solution)/shard_map/ppermute | solution.py:28
  58.0 10.1 %all-to-all-start.1 = ((bf16[16,16,128]{2,1,0:T(8,128)(2,1)}), bf16[16,16,128]{2,1,0:T(8,128)(2,1)S(1)}, u32[]{:S(2)}, u32[]{:S(2)}) async-start(bf16[16,16,128]{2,1,0:T(8,128)(2,1)} %get-tuple-element.50), calls=%async_computation.1 | async-start | bytes 131072 | tf_op jit(solution)/shard_map/all_to_all | solution.py:274
where the time goes:
time: 70.5 us; the launch traced here: 70.1 us
  starting transfers between devices  25 us (35%)
  Pallas kernels  23.7 us (34%)
  blocking collectives  11.2 us (16%)
  waiting for transfers between devices  9.4 us (13%)
  between operations  0.76 us (1%)
    ppermute x18, starting transfers between devices, shift(): return lax.ppermute(x, axis, [(i, dest(i, s, n)) for i in range(n)])  21.5 us
    pallas_call x5, Pallas kernels, kernel_call(): pl.pallas_call(body, out_shape=[o.array if isinstance(o, Far) else o if i...  19.3 us
    all_to_all x1, blocking collectives, shards(): gathered = lax.all_to_all(out[0], ('dp', 'tp'), 0, 0, tiled=True)  11.2 us
    ppermute x18, waiting for transfers between devices, shift(): return lax.ppermute(x, axis, [(i, dest(i, s, n)) for i in range(n)])  7.28 us
    pallas_call x1, Pallas kernels, shards(): pl.pallas_call(functools.partial(write_body, blocks=blocks, span=span), o...  4.46 us
    all_to_all x1, starting transfers between devices, shards(): gathered = lax.all_to_all(out[0], ('dp', 'tp'), 0, 0, tiled=True)  3.5 us
    all_to_all x1, waiting for transfers between devices, shards(): gathered = lax.all_to_all(out[0], ('dp', 'tp'), 0, 0, tiled=True)  2.12 us
  transfers between devices with their start and end apart: 19, of which 8 were waited for; matrix products, arithmetic and copies ran while one was open for 0% of the time, Pallas kernels for 14%

commit v1 on v0

--- a/solution.py
+++ b/solution.py
@@ -171,20 +171,16 @@
     stab_out[...] = jnp.broadcast_to(new_stab, stab_out.shape)
 
 
-def write_body(mem_ref, norm_ref, *refs, blocks, span):
-    given, (mem_out, norm_out, stab_out) = refs[:4 * blocks], refs[4 * blocks:]
-    for blk in range(blocks):
-        @pl.when(pl.program_id(0) == blk)
-        def _(blk=blk):
-            keep_ref, added_ref, value_ref, stab_ref = given[4 * blk:4 * blk + 4]
-            rows = pl.ds(pl.multiple_of(pl.program_id(1) * span, span), span)
-            keep, added, value = keep_ref[rows, :], added_ref[rows, :], value_ref[rows, :]
-            added_t = added.T
-            for s in range(span):
-                mem_out[0, s, 0] = (
-                    keep[s:s + 1, :] * mem_ref[0, s, 0] + added_t[:, s:s + 1] * value[s:s + 1, :])
-            norm_out[0, :, 0, :] = keep * norm_ref[0, :, 0, :] + added
-            stab_out[0] = stab_ref[...].T[0:1, :]
+def write_body(mem_ref, norm_ref, keep_ref, added_ref, value_ref, stab_ref, *refs, span):
+    mem_out, norm_out, stab_out = refs[-3:]
+    rows = pl.ds(pl.multiple_of(pl.program_id(0) * span, span), span)
+    keep, added, value = keep_ref[rows, :], added_ref[rows, :], value_ref[rows, :]
+    added_t = added.T
+    for s in range(span):
+        mem_out[0, s, 0] = (
+            keep[s:s + 1, :] * mem_ref[0, s, 0] + added_t[:, s:s + 1] * value[s:s + 1, :])
+    norm_out[0, :, 0, :] = keep * norm_ref[0, :, 0, :] + added
+    stab_out[0] = stab_ref[...].T[0:1, :]
 
 
 VMEM = pl.BlockSpec(memory_space=pltpu.VMEM)
@@ -216,6 +212,24 @@
         scratch_shapes=list(scratch),
     )(*scalars, *(t.array if isinstance(t, Far) else near(t, room or t.nbytes < NEAR_BYTES // 32) for t in ins))
     return list(out)
+
+
+def write_state(memory, normalizer, stab_t, given, states, blk):
+    seq_own, dk = memory.shape[1], memory.shape[-1]
+    span = seq_own // 2
+    specs = [
+        pl.BlockSpec((1, span, 1, dk, dk), lambda c: (blk, c, 0, 0, 0)),
+        pl.BlockSpec((1, span, 1, dk), lambda c: (blk, c, 0, 0))]
+    states = [] if states is None else states
+    return pl.pallas_call(
+        functools.partial(write_body, span=span),
+        out_shape=[jax.ShapeDtypeStruct(t.shape, t.dtype) for t in (memory, normalizer, stab_t)],
+        grid=(seq_own // span,),
+        in_specs=specs + [VMEM] * len(given) + [ANY] * len(states),
+        out_specs=specs + [pl.BlockSpec((1, 1, seq_own), lambda c: (blk, 0, 0))],
+        input_output_aliases={2 + len(given) + a: a for a in range(len(states))},
+        name="write_state",
+    )(memory, normalizer, *(near(t, True) for t in given), *states)
 
 
 def shards(tokens, norm_gain, w_query, w_key, w_value, w_outgate, gate_weight, forget_bias, w_mix,
@@ -244,13 +258,13 @@
     out = kernel_call(
         functools.partial(first_body, n_dp=n_dp, n_grp=n_grp, seq_own=seq_own),
         [Far(tokens), far_gain, *weights, far_mix],
-        part_shapes + [Far(jax.ShapeDtypeStruct((w_mix.shape[1], feats // n_grp), w_mix.dtype))] * blocks,
+        part_shapes + [((w_mix.shape[1], feats // n_grp), w_mix.dtype)],
         [buf, stage, x_buf, gain_buf, sems])
-    parts, own_mixes = out[:n_dp], out[n_dp:]
+    parts, own = out[:n_dp], out[n_dp]
 
     x = tokens
     given = []
-    gathered = None
+    gathered = states = None
     for blk in range(blocks):
         if gathered is not None:
             out = kernel_call(
@@ -259,10 +273,8 @@
                 [jax.ShapeDtypeStruct(*x_shape)] + part_shapes, [acc, own_mix, buf, stage, x_buf, gain_buf, sems])
             x, parts = out[0], out[1:]
         arrived = [parts[0]] + [shift(parts[s], "dp", s, n_dp) for s in range(1, n_dp)]
-        own = own_mixes[blk]
-        if gathered is not None:
-            own, _ = lax.optimization_barrier((own, x))
-        pieces = [shift(own, "tp", s, n_tp) for s in range(1, n_tp)]
+        if gathered is None:
+            pieces = [shift(own, "tp", s, n_tp) for s in range(1, n_tp)]
         small = ((seq_own, dk), jnp.float32)
         out = kernel_call(
             functools.partial(cell_body, blk=blk, n_dp=n_dp, width=feats * n_dp, copies=n_dp * n_tp),
@@ -270,25 +282,20 @@
             [((n_dp * n_tp, seq_own, dk), jnp.bfloat16)] + [small] * 4,
             [pltpu.VMEM((seq_own, dk, dk), memory.dtype), pltpu.SemaphoreType.DMA((4,))],
             scalars=(bias_t,))
-        given += out[1:]
+        given = out[1:]
         gathered = lax.all_to_all(out[0], ("dp", "tp"), 0, 0, tiled=True)
         gathered = gathered.reshape(n_dp, n_tp, seq_own, dk)
         mixes = []
         for piece in pieces:
             piece, _ = lax.optimization_barrier((piece, out[1]))
             mixes += [piece] + [shift(piece, "grp", h, n_grp) for h in range(1, n_grp)]
-    span = seq_own // 2
-    state_specs = [
-        pl.BlockSpec((1, span, 1, dk, dk), lambda b, c: (b, c, 0, 0, 0)),
-        pl.BlockSpec((1, span, 1, dk), lambda b, c: (b, c, 0, 0))]
-    new_mem, new_norm, new_stab = pl.pallas_call(
-        functools.partial(write_body, blocks=blocks, span=span),
-        out_shape=[jax.ShapeDtypeStruct(t.shape, t.dtype) for t in (memory, normalizer, stab_t)],
-        grid=(blocks, seq_own // span),
-        in_specs=state_specs + [VMEM] * len(given),
-        out_specs=state_specs + [pl.BlockSpec((1, 1, seq_own), lambda b, c: (b, 0, 0))],
-        name="write_state",
-    )(memory, normalizer, *(near(t, True) for t in given))
+        if blk + 1 < blocks:
+            part = lax.axis_index("grp") * (feats // n_grp)
+            own = lax.dynamic_slice_in_dim(w_mix[blk + 1], part, feats // n_grp, 1)
+            own, _ = lax.optimization_barrier((own, gathered))
+            pieces = [shift(own, "tp", s, n_tp) for s in range(1, n_tp)]
+        states = write_state(memory, normalizer, stab_t, given, states, blk)
+    new_mem, new_norm, new_stab = states
     (x,) = kernel_call(
         functools.partial(last_body, blk=blocks - 1, **sizes),
         [Far(x), gathered, far_mix, *mixes], [x_shape], [acc, own_mix, x_buf, sems],

time: 70.5 us -> 60.5 us (0.86)
  blocking collectives: 11.2 us -> 0 us
  Pallas kernels: 23.7 us -> 17.7 us
  starting transfers between devices: 25 us -> 29.8 us
  waiting for transfers between devices: 9.4 us -> 11.8 us
    all_to_all x1 -> x0, blocking collectives: 11.2 us -> none  [shards(): gathered = lax.all_to_all(out[0], ('dp', 'tp'), 0, 0, tiled=True)]
    pallas_call x5, Pallas kernels: 19.3 us -> 12.6 us  [kernel_call(): pl.pallas_call(body, out_shape=[o.array if isinstance(o, Far) else o if i...]
    all_to_all x1 -> x2, starting transfers between devices: 3.5 us -> 9.2 us  [shards(): gathered = lax.all_to_all(out[0], ('dp', 'tp'), 0, 0, tiled=True)]
    all_to_all x1 -> x2, waiting for transfers between devices: 2.12 us -> 6.01 us  [shards(): gathered = lax.all_to_all(out[0], ('dp', 'tp'), 0, 0, tiled=True)]
    ppermute x18, waiting for transfers between devices: 7.28 us -> 5.78 us  [shift(): return lax.ppermute(x, axis, [(i, dest(i, s, n)) for i in range(n)])]
    ppermute x18, starting transfers between devices: 21.5 us -> 20.6 us  [shift(): return lax.ppermute(x, axis, [(i, dest(i, s, n)) for i in range(n)])]
    pallas_call x1 -> x2, Pallas kernels: 4.46 us -> 5.07 us  [write_state(): pl.pallas_call(functools.partial(write_body, span=span), out_shape=[jax.S...]
  transfers between devices with their start and end apart: 19 -> 20, of which waited for: 8 -> 7; matrix products, arithmetic and copies ran while one was open for 0% -> 0% of each run, Pallas kernels for 14% -> 23%
where the time goes in v1:
time: 60.5 us; the launch traced here: 60.1 us
  starting transfers between devices  29.8 us (49%)
  Pallas kernels  17.7 us (29%)
  waiting for transfers between devices  11.8 us (20%)
  between operations  0.79 us (1%)
    ppermute x18, starting transfers between devices, shift(): return lax.ppermute(x, axis, [(i, dest(i, s, n)) for i in range(n)])  20.6 us
    pallas_call x5, Pallas kernels, kernel_call(): pl.pallas_call(body, out_shape=[o.array if isinstance(o, Far) else o if i...  12.6 us
    all_to_all x2, starting transfers between devices, shards(): gathered = lax.all_to_all(out[0], ('dp', 'tp'), 0, 0, tiled=True)  9.2 us
    all_to_all x2, waiting for transfers between devices, shards(): gathered = lax.all_to_all(out[0], ('dp', 'tp'), 0, 0, tiled=True)  6.01 us
    ppermute x18, waiting for transfers between devices, shift(): return lax.ppermute(x, axis, [(i, dest(i, s, n)) for i in range(n)])  5.78 us
    pallas_call x2, Pallas kernels, write_state(): pl.pallas_call(functools.partial(write_body, span=span), out_shape=[jax.S...  5.07 us
  transfers between devices with their start and end apart: 20, of which 7 were waited for; matrix products, arithmetic and copies ran while one was open for 0% of the time, Pallas kernels for 23%

profile of v1, /device:TPU:0, one launch (start us, length us, event | category | flops | bytes accessed | tf_op | source)
XLA Modules:
  0.0 60.1 jit_solution(6409499156033131125)
XLA Ops:
  0.6 0.0 copy-start
  0.7 1.9 %shard_map.147 = (f32[16,640]{1,0:T(8,128)S(1)}, f32[16,640]{1,0:T(8,128)S(1)}, f32[16,640]{1,0:T(8,128)S(1)}, f32[16,640]{1,0:T(8,128)S(1)}, bf16[128,512]{1,0:T(8,128)(2,1)S(1)}) custom-call(bf16[64,1024]{1,0:T(8,128)(2,1)} %x_ref.3, f32[2,1024]{1,0:T(2,128)} %rest_6_.1, bf16[2,1024,128]{2,1,0:T(8,128)(2,1)} %rest_7_.1, bf16[2,1024,128]{2,1,0:T(8,128)(2,1)} %rest_8_.1, ...), custom_call_target="tpu_custom_call" | custom-call | tf_op jit(solution)/shard_map/pallas_call | solution.py:205
  2.5 0.0 slice-start
  2.5 5.1 %collective-permute-start.7 = (bf16[128,512]{1,0:T(8,128)(2,1)S(1)}, bf16[128,512]{1,0:T(8,128)(2,1)S(1)}, u32[]{:S(2)}, u32[]{:S(2)}) collective-permute-start(bf16[128,512]{1,0:T(8,128)(2,1)S(1)} %get-tuple-element.42), channel_id=1, source_target_pairs={{0,12},{4,8},{8,4},{12,0},{1,13},{5,9},{9,5},{13,1},{2,14},{6,10},... | collective-permute-start | bytes 393224 | tf_op jit(solution)/shard_map/ppermute | solution.py:28
  7.7 0.0 collective-permute-start.5
  7.7 0.6 %collective-permute-start.3 = (bf16[128,512]{1,0:T(8,128)(2,1)S(1)}, bf16[128,512]{1,0:T(8,128)(2,1)S(1)}, u32[]{:S(2)}, u32[]{:S(2)}) collective-permute-start(bf16[128,512]{1,0:T(8,128)(2,1)S(1)} %get-tuple-element.42), channel_id=1, source_target_pairs={{0,4},{4,0},{8,12},{12,8},{1,5},{5,1},{9,13},{13,9},{2,6},{6,2},{1... | collective-permute-start | bytes 393224 | tf_op jit(solution)/shard_map/ppermute | solution.py:28
  8.3 0.0 collective-permute-start
  8.3 1.6 %collective-permute-start.1 = (f32[16,640]{1,0:T(8,128)S(1)}, f32[16,640]{1,0:T(8,128)S(1)}, u32[]{:S(2)}, u32[]{:S(2)}) collective-permute-start(f32[16,640]{1,0:T(8,128)S(1)} %get-tuple-element.39), channel_id=1, source_target_pairs={{0,2},{1,3},{2,0},{3,1},{4,6},{5,7},{6,4},{7,5},{8,10},{9,11},{10,... | collective-permute-start | bytes 122888 | tf_op jit(solution)/shard_map/ppermute | solution.py:28
  10.0 0.0 collective-permute-done.refs_1_
  10.0 1.0 %collective-permute-start.2 = (f32[16,640]{1,0:T(8,128)S(1)}, f32[16,640]{1,0:T(8,128)S(1)}, u32[]{:S(2)}, u32[]{:S(2)}) collective-permute-start(f32[16,640]{1,0:T(8,128)S(1)} %get-tuple-element.40), channel_id=1, source_target_pairs={{0,3},{1,2},{2,1},{3,0},{4,7},{5,6},{6,5},{7,4},{8,11},{9,10},{10,... | collective-permute-start | bytes 122888 | tf_op jit(solution)/shard_map/ppermute | solution.py:28
  10.9 1.4 %collective-permute-done.1.refs_2_ = f32[16,640]{1,0:T(8,128)S(1)} collective-permute-done((f32[16,640]{1,0:T(8,128)S(1)}, f32[16,640]{1,0:T(8,128)S(1)}, u32[]{:S(2)}, u32[]{:S(2)}) %collective-permute-start.1) | collective-permute-done | bytes 40992 | tf_op jit(solution)/shard_map/ppermute | solution.py:28
  12.3 1.1 %collective-permute-done.2.refs_3_ = f32[16,640]{1,0:T(8,128)S(1)} collective-permute-done((f32[16,640]{1,0:T(8,128)S(1)}, f32[16,640]{1,0:T(8,128)S(1)}, u32[]{:S(2)}, u32[]{:S(2)}) %collective-permute-start.2) | collective-permute-done | bytes 40992 | tf_op jit(solution)/shard_map/ppermute | solution.py:28
  13.4 3.2 %shard_map.148 = (bf16[16,16,128]{2,1,0:T(8,128)(2,1)}, f32[16,128]{1,0:T(8,128)S(1)}, f32[16,128]{1,0:T(8,128)S(1)}, f32[16,128]{1,0:T(8,128)S(1)}, f32[16,128]{1,0:T(8,128)S(1)}) custom-call(f32[1,2]{1,0:T(1,128)} %bitcast.18, f32[16,640]{1,0:T(8,128)S(1)} %get-tuple-element.37.refs_0_, f32[16,640]{1,0:T(8,128)S(1)} %collective-permute-done.refs_1_, ...), custom_call_target="tpu_custom_call" | custom-call | tf_op jit(solution)/shard_map/pallas_call | solution.py:205
  16.7 0.0 collective-permute-done.7.rest_4_
  16.7 1.6 %collective-permute-start.8 = (bf16[128,512]{1,0:T(8,128)(2,1)S(1)}, bf16[128,512]{1,0:T(8,128)(2,1)S(1)}, u32[]{:S(2)}, u32[]{:S(2)}) collective-permute-start(bf16[128,512]{1,0:T(8,128)(2,1)S(1)} %collective-permute-done.7.rest_4_), channel_id=1, source_target_pairs={{0,16},{16,0},{1,17},{17,1},{2,18},{18,2},{3,19},{19,3},{4,20},{20... | collective-permute-start | bytes 393224 | tf_op jit(solution)/shard_map/ppermute | solution.py:28
  18.3 5.7 %all-to-all-start = ((bf16[16,16,128]{2,1,0:T(8,128)(2,1)}), bf16[16,16,128]{2,1,0:T(8,128)(2,1)S(1)}, u32[]{:S(2)}, u32[]{:S(2)}) async-start(bf16[16,16,128]{2,1,0:T(8,128)(2,1)} %get-tuple-element.41), calls=%async_computation | async-start | bytes 131072 | tf_op jit(solution)/shard_map/all_to_all | solution.py:286
  24.0 0.0 collective-permute-done.5.rest_2_
  24.0 0.6 collective-permute-start.6
  24.6 0.0 collective-permute-done.3.rest_0_
  24.6 1.5 %collective-permute-start.4 = (bf16[128,512]{1,0:T(8,128)(2,1)S(1)}, bf16[128,512]{1,0:T(8,128)(2,1)S(1)}, u32[]{:S(2)}, u32[]{:S(2)}) collective-permute-start(bf16[128,512]{1,0:T(8,128)(2,1)S(1)} %collective-permute-done.3.rest_0_), channel_id=1, source_target_pairs={{0,16},{16,0},{1,17},{17,1},{2,18},{18,2},{3,19},{19,3},{4,20},{20... | collective-permute-start | bytes 393224 | tf_op jit(solution)/shard_map/ppermute | solution.py:28
  26.1 4.5 %all-to-all-done = bf16[16,16,128]{2,1,0:T(8,128)(2,1)S(1)} async-done(((bf16[16,16,128]{2,1,0:T(8,128)(2,1)}), bf16[16,16,128]{2,1,0:T(8,128)(2,1)S(1)}, u32[]{:S(2)}, u32[]{:S(2)}) %all-to-all-start) | async-done | bytes 65568 | tf_op jit(solution)/shard_map/all_to_all | solution.py:286
  30.6 0.7 %collective-permute-start.16 = (bf16[128,512]{1,0:T(8,128)(2,1)S(1)}, bf16[128,512]{1,0:T(8,128)(2,1)S(1)}, u32[]{:S(2)}, u32[]{:S(2)}) collective-permute-start(bf16[128,512]{1,0:T(8,128)(2,1)S(1)} %dynamic-slice_bitcast_fusion), channel_id=1, source_target_pairs={{0,12},{4,8},{8,4},{12,0},{1,13},{5,9},{9,5},{13,1},{2,14},{6,10},... | collective-permute-start | bytes 393224 | tf_op jit(solution)/shard_map/ppermute | solution.py:28
  31.4 1.1 %collective-permute-start.14 = (bf16[128,512]{1,0:T(8,128)(2,1)S(1)}, bf16[128,512]{1,0:T(8,128)(2,1)S(1)}, u32[]{:S(2)}, u32[]{:S(2)}) collective-permute-start(bf16[128,512]{1,0:T(8,128)(2,1)S(1)} %dynamic-slice_bitcast_fusion), channel_id=1, source_target_pairs={{0,8},{4,12},{8,0},{12,4},{1,9},{5,13},{9,1},{13,5},{2,10},{6,14},... | collective-permute-start | bytes 393224 | tf_op jit(solution)/shard_map/ppermute | solution.py:28
  32.4 0.0 collective-permute-done.8.rest_5_
  32.4 2.6 %collective-permute-start.12 = (bf16[128,512]{1,0:T(8,128)(2,1)S(1)}, bf16[128,512]{1,0:T(8,128)(2,1)S(1)}, u32[]{:S(2)}, u32[]{:S(2)}) collective-permute-start(bf16[128,512]{1,0:T(8,128)(2,1)S(1)} %dynamic-slice_bitcast_fusion), channel_id=1, source_target_pairs={{0,4},{4,0},{8,12},{12,8},{1,5},{5,1},{9,13},{13,9},{2,6},{6,2},{1... | collective-permute-start | bytes 393224 | tf_op jit(solution)/shard_map/ppermute | solution.py:28
  35.0 0.0 collective-permute-done.6.rest_3_
  35.0 0.0 collective-permute-done.4.rest_1_
  35.0 2.6 %shard_map.149 = (bf16[64,1024]{1,0:T(8,128)(2,1)}, f32[16,640]{1,0:T(8,128)S(1)}, f32[16,640]{1,0:T(8,128)S(1)}, f32[16,640]{1,0:T(8,128)S(1)}, f32[16,640]{1,0:T(8,128)S(1)}) custom-call(bf16[64,1024]{1,0:T(8,128)(2,1)} %x_ref.3, bf16[4,4,16,128]{3,2,1,0:T(8,128)(2,1)S(1)} %bitcast.12, bf16[2,128,1024]{2,1,0:T(8,128)(2,1)} %mix_ref.5, ...), custom_call_target="tpu_custom_call" | custom-call | tf_op jit(solution)/shard_map/pallas_call | solution.py:205
  37.6 0.1 collective-permute-start.9
  37.7 0.8 %collective-permute-start.10 = (f32[16,640]{1,0:T(8,128)S(1)}, f32[16,640]{1,0:T(8,128)S(1)}, u32[]{:S(2)}, u32[]{:S(2)}) collective-permute-start(f32[16,640]{1,0:T(8,128)S(1)} %get-tuple-element.50), channel_id=1, source_target_pairs={{0,2},{1,3},{2,0},{3,1},{4,6},{5,7},{6,4},{7,5},{8,10},{9,11},{10,... | collective-permute-start | bytes 122888 | tf_op jit(solution)/shard_map/ppermute | solution.py:28
  38.5 0.4 collective-permute-done.9.refs_1_
  38.9 0.6 %collective-permute-start.11 = (f32[16,640]{1,0:T(8,128)S(1)}, f32[16,640]{1,0:T(8,128)S(1)}, u32[]{:S(2)}, u32[]{:S(2)}) collective-permute-start(f32[16,640]{1,0:T(8,128)S(1)} %get-tuple-element.51), channel_id=1, source_target_pairs={{0,3},{1,2},{2,1},{3,0},{4,7},{5,6},{6,5},{7,4},{8,11},{9,10},{10,... | collective-permute-start | bytes 122888 | tf_op jit(solution)/shard_map/ppermute | solution.py:28
  39.5 2.2 %collective-permute-done.10.refs_2_ = f32[16,640]{1,0:T(8,128)S(1)} collective-permute-done((f32[16,640]{1,0:T(8,128)S(1)}, f32[16,640]{1,0:T(8,128)S(1)}, u32[]{:S(2)}, u32[]{:S(2)}) %collective-permute-start.10) | collective-permute-done | bytes 40992 | tf_op jit(solution)/shard_map/ppermute | solution.py:28
  41.8 0.7 %collective-permute-done.11.refs_3_ = f32[16,640]{1,0:T(8,128)S(1)} collective-permute-done((f32[16,640]{1,0:T(8,128)S(1)}, f32[16,640]{1,0:T(8,128)S(1)}, u32[]{:S(2)}, u32[]{:S(2)}) %collective-permute-start.11) | collective-permute-done | bytes 40992 | tf_op jit(solution)/shard_map/ppermute | solution.py:28
  42.4 2.9 %shard_map.150 = (bf16[16,16,128]{2,1,0:T(8,128)(2,1)}, f32[16,128]{1,0:T(8,128)S(1)}, f32[16,128]{1,0:T(8,128)S(1)}, f32[16,128]{1,0:T(8,128)S(1)}, f32[16,128]{1,0:T(8,128)S(1)}) custom-call(f32[1,2]{1,0:T(1,128)} %bitcast.19, f32[16,640]{1,0:T(8,128)S(1)} %get-tuple-element.48.refs_0_, f32[16,640]{1,0:T(8,128)S(1)} %collective-permute-done.9.refs_1_, ...), custom_call_target="tpu_custom_call" | custom-call | tf_op jit(solution)/shard_map/pallas_call | solution.py:205
  45.3 0.0 collective-permute-done.16.rest_4_
  45.3 0.0 collective-permute-done.14.rest_2_
  45.3 0.6 collective-permute-start.13
  45.9 1.5 %collective-permute-start.15 = (bf16[128,512]{1,0:T(8,128)(2,1)S(1)}, bf16[128,512]{1,0:T(8,128)(2,1)S(1)}, u32[]{:S(2)}, u32[]{:S(2)}) collective-permute-start(bf16[128,512]{1,0:T(8,128)(2,1)S(1)} %collective-permute-done.14.rest_2_), channel_id=1, source_target_pairs={{0,16},{16,0},{1,17},{17,1},{2,18},{18,2},{3,19},{19,3},{4,20},{20... | collective-permute-start | bytes 393224 | tf_op jit(solution)/shard_map/ppermute | solution.py:28
  47.4 0.5 collective-permute-start.17
  48.0 3.5 %all-to-all-start.1 = ((bf16[16,16,128]{2,1,0:T(8,128)(2,1)}), bf16[16,16,128]{2,1,0:T(8,128)(2,1)S(1)}, u32[]{:S(2)}, u32[]{:S(2)}) async-start(bf16[16,16,128]{2,1,0:T(8,128)(2,1)} %get-tuple-element.52), calls=%async_computation.1 | async-start | bytes 131072 | tf_op jit(solution)/shard_map/all_to_all | solution.py:286
  51.5 2.5 %write_state.2 = (f32[2,16,1,128,128]{4,3,2,1,0:T(8,128)}, f32[2,16,1,128]{3,2,1,0:T(1,128)}, f32[2,1,16]{2,1,0:T(1,128)}) custom-call(f32[2,16,1,128,128]{4,3,2,1,0:T(8,128)} %mem_ref.3, f32[2,16,1,128]{3,2,1,0:T(1,128)} %norm_ref.3, f32[16,128]{1,0:T(8,128)S(1)} %get-tuple-element.43.keep_ref, f32[16,128]{1,0:T(8,128)S(1)} %get-tuple-element.61.added_ref, ...), custom_call_target="tpu_custom_call" | custom-call | tf_op jit(solution)/shard_map/write_state/pallas_call | solution.py:224
  54.0 2.5 %write_state.3 = (f32[2,16,1,128,128]{4,3,2,1,0:T(8,128)}, f32[2,16,1,128]{3,2,1,0:T(1,128)}, f32[2,1,16]{2,1,0:T(1,128)}) custom-call(f32[2,16,1,128,128]{4,3,2,1,0:T(8,128)} %mem_ref.3, f32[2,16,1,128]{3,2,1,0:T(1,128)} %norm_ref.3, f32[16,128]{1,0:T(8,128)S(1)} %get-tuple-element.54.keep_ref, ...), custom_call_target="tpu_custom_call", output_to_operand_aliasing={{0}: (6, {}), {1}: (7, {}), {2}: (8, {})} | custom-call | tf_op jit(solution)/shard_map/write_state/pallas_call | solution.py:224
  56.5 1.5 %all-to-all-done.1 = bf16[16,16,128]{2,1,0:T(8,128)(2,1)S(1)} async-done(((bf16[16,16,128]{2,1,0:T(8,128)(2,1)}), bf16[16,16,128]{2,1,0:T(8,128)(2,1)S(1)}, u32[]{:S(2)}, u32[]{:S(2)}) %all-to-all-start.1) | async-done | bytes 65568 | tf_op jit(solution)/shard_map/all_to_all | solution.py:286
  58.0 0.0 collective-permute-done.13.rest_1_
  58.0 0.0 collective-permute-done.15.rest_3_
  58.0 0.0 collective-permute-done.17.rest_5_
  58.1 2.0 %shard_map.151 = bf16[64,1024]{1,0:T(8,128)(2,1)} custom-call(bf16[64,1024]{1,0:T(8,128)(2,1)} %get-tuple-element.47.x_ref, bf16[4,4,16,128]{3,2,1,0:T(8,128)(2,1)S(1)} %bitcast.13, bf16[2,128,1024]{2,1,0:T(8,128)(2,1)} %mix_ref.5, bf16[128,512]{1,0:T(8,128)(2,1)S(1)} %collective-permute-done.12.rest_0_, ...), custom_call_target="tpu_custom_call" | custom-call | tf_op jit(solution)/shard_map/pallas_call | solution.py:205
  (8 shorter events, 0.0 us)
Async XLA Ops:
  0.6 12.8 %copy-start = (f32[2,16,1,128]{3,2,1,0:T(1,128)S(1)}, f32[2,16,1,128]{3,2,1,0:T(1,128)}, u32[]{:S(2)}) copy-start(f32[2,16,1,128]{3,2,1,0:T(1,128)} %norm_ref.3) | copy-start | bytes 49156
  0.6 12.8 %copy-start.2 = (f32[2,16,1]{1,2,0:T(1,128)S(1)}, f32[2,16,1]{1,2,0:T(1,128)}, u32[]{:S(2)}) copy-start(f32[2,16,1]{1,2,0:T(1,128)} %param.23) | copy-start | bytes 388
  0.7 12.8 %copy-start.1 = (bf16[2,1,384,2]{2,3,1,0:T(2,128)(2,1)S(1)}, bf16[2,1,384,2]{2,3,1,0:T(2,128)(2,1)}, u32[]{:S(2)}) copy-start(bf16[2,1,384,2]{2,3,1,0:T(2,128)(2,1)} %param.18) | copy-start | bytes 9220
  2.5 23.6 %slice-start = ((bf16[2,128,1024]{2,1,0:T(8,128)(2,1)}), bf16[1,128,1024]{2,1,0:T(8,128)(2,1)S(1)}, s32[]{:S(2)}) async-start(bf16[2,128,1024]{2,1,0:T(8,128)(2,1)} %mix_ref.5), calls=%async_computation.2 | async-start | bytes 524288 | tf_op jit(solution)/shard_map/slice | solution.py:294
  2.5 14.1 %collective-permute-start.7 = (bf16[128,512]{1,0:T(8,128)(2,1)S(1)}, bf16[128,512]{1,0:T(8,128)(2,1)S(1)}, u32[]{:S(2)}, u32[]{:S(2)}) collective-permute-start(bf16[128,512]{1,0:T(8,128)(2,1)S(1)} %get-tuple-element.42), channel_id=1, source_target_pairs={{0,12},{4,8},{8,4},{12,0},{1,13},{5,9},{9,5},{13,1},{2,14},{6,10},... | collective-permute-start | bytes 393224 | tf_op jit(solution)/shard_map/ppermute | solution.py:28
  7.7 16.3 %collective-permute-start.5 = (bf16[128,512]{1,0:T(8,128)(2,1)S(1)}, bf16[128,512]{1,0:T(8,128)(2,1)S(1)}, u32[]{:S(2)}, u32[]{:S(2)}) collective-permute-start(bf16[128,512]{1,0:T(8,128)(2,1)S(1)} %get-tuple-element.42), channel_id=1, source_target_pairs={{0,8},{4,12},{8,0},{12,4},{1,9},{5,13},{9,1},{13,5},{2,10},{6,14},... | collective-permute-start | bytes 393224 | tf_op jit(solution)/shard_map/ppermute | solution.py:28
  7.7 16.9 %collective-permute-start.3 = (bf16[128,512]{1,0:T(8,128)(2,1)S(1)}, bf16[128,512]{1,0:T(8,128)(2,1)S(1)}, u32[]{:S(2)}, u32[]{:S(2)}) collective-permute-start(bf16[128,512]{1,0:T(8,128)(2,1)S(1)} %get-tuple-element.42), channel_id=1, source_target_pairs={{0,4},{4,0},{8,12},{12,8},{1,5},{5,1},{9,13},{13,9},{2,6},{6,2},{1... | collective-permute-start | bytes 393224 | tf_op jit(solution)/shard_map/ppermute | solution.py:28
  8.3 1.6 %collective-permute-start = (f32[16,640]{1,0:T(8,128)S(1)}, f32[16,640]{1,0:T(8,128)S(1)}, u32[]{:S(2)}, u32[]{:S(2)}) collective-permute-start(f32[16,640]{1,0:T(8,128)S(1)} %get-tuple-element.38), channel_id=1, source_target_pairs={{0,1},{1,0},{2,3},{3,2},{4,5},{5,4},{6,7},{7,6},{8,9},{9,8},{10,11... | collective-permute-start | bytes 122888 | tf_op jit(solution)/shard_map/ppermute | solution.py:28
  8.3 4.0 %collective-permute-start.1 = (f32[16,640]{1,0:T(8,128)S(1)}, f32[16,640]{1,0:T(8,128)S(1)}, u32[]{:S(2)}, u32[]{:S(2)}) collective-permute-start(f32[16,640]{1,0:T(8,128)S(1)} %get-tuple-element.39), channel_id=1, source_target_pairs={{0,2},{1,3},{2,0},{3,1},{4,6},{5,7},{6,4},{7,5},{8,10},{9,11},{10,... | collective-permute-start | bytes 122888 | tf_op jit(solution)/shard_map/ppermute | solution.py:28
  10.0 3.5 %collective-permute-start.2 = (f32[16,640]{1,0:T(8,128)S(1)}, f32[16,640]{1,0:T(8,128)S(1)}, u32[]{:S(2)}, u32[]{:S(2)}) collective-permute-start(f32[16,640]{1,0:T(8,128)S(1)} %get-tuple-element.40), channel_id=1, source_target_pairs={{0,3},{1,2},{2,1},{3,0},{4,7},{5,6},{6,5},{7,4},{8,11},{9,10},{10,... | collective-permute-start | bytes 122888 | tf_op jit(solution)/shard_map/ppermute | solution.py:28
  16.7 15.7 %collective-permute-start.8 = (bf16[128,512]{1,0:T(8,128)(2,1)S(1)}, bf16[128,512]{1,0:T(8,128)(2,1)S(1)}, u32[]{:S(2)}, u32[]{:S(2)}) collective-permute-start(bf16[128,512]{1,0:T(8,128)(2,1)S(1)} %collective-permute-done.7.rest_4_), channel_id=1, source_target_pairs={{0,16},{16,0},{1,17},{17,1},{2,18},{18,2},{3,19},{19,3},{4,20},{20... | collective-permute-start | bytes 393224 | tf_op jit(solution)/shard_map/ppermute | solution.py:28
  18.3 12.3 %all-to-all-start = ((bf16[16,16,128]{2,1,0:T(8,128)(2,1)}), bf16[16,16,128]{2,1,0:T(8,128)(2,1)S(1)}, u32[]{:S(2)}, u32[]{:S(2)}) async-start(bf16[16,16,128]{2,1,0:T(8,128)(2,1)} %get-tuple-element.41), calls=%async_computation | async-start | bytes 131072 | tf_op jit(solution)/shard_map/all_to_all | solution.py:286
  24.0 11.0 %collective-permute-start.6 = (bf16[128,512]{1,0:T(8,128)(2,1)S(1)}, bf16[128,512]{1,0:T(8,128)(2,1)S(1)}, u32[]{:S(2)}, u32[]{:S(2)}) collective-permute-start(bf16[128,512]{1,0:T(8,128)(2,1)S(1)} %collective-permute-done.5.rest_2_), channel_id=1, source_target_pairs={{0,16},{16,0},{1,17},{17,1},{2,18},{18,2},{3,19},{19,3},{4,20},{20... | collective-permute-start | bytes 393224 | tf_op jit(solution)/shard_map/ppermute | solution.py:28
  24.6 10.4 %collective-permute-start.4 = (bf16[128,512]{1,0:T(8,128)(2,1)S(1)}, bf16[128,512]{1,0:T(8,128)(2,1)S(1)}, u32[]{:S(2)}, u32[]{:S(2)}) collective-permute-start(bf16[128,512]{1,0:T(8,128)(2,1)S(1)} %collective-permute-done.3.rest_0_), channel_id=1, source_target_pairs={{0,16},{16,0},{1,17},{17,1},{2,18},{18,2},{3,19},{19,3},{4,20},{20... | collective-permute-start | bytes 393224 | tf_op jit(solution)/shard_map/ppermute | solution.py:28
  30.6 14.7 %collective-permute-start.16 = (bf16[128,512]{1,0:T(8,128)(2,1)S(1)}, bf16[128,512]{1,0:T(8,128)(2,1)S(1)}, u32[]{:S(2)}, u32[]{:S(2)}) collective-permute-start(bf16[128,512]{1,0:T(8,128)(2,1)S(1)} %dynamic-slice_bitcast_fusion), channel_id=1, source_target_pairs={{0,12},{4,8},{8,4},{12,0},{1,13},{5,9},{9,5},{13,1},{2,14},{6,10},... | collective-permute-start | bytes 393224 | tf_op jit(solution)/shard_map/ppermute | solution.py:28
  31.4 14.0 %collective-permute-start.14 = (bf16[128,512]{1,0:T(8,128)(2,1)S(1)}, bf16[128,512]{1,0:T(8,128)(2,1)S(1)}, u32[]{:S(2)}, u32[]{:S(2)}) collective-permute-start(bf16[128,512]{1,0:T(8,128)(2,1)S(1)} %dynamic-slice_bitcast_fusion), channel_id=1, source_target_pairs={{0,8},{4,12},{8,0},{12,4},{1,9},{5,13},{9,1},{13,5},{2,10},{6,14},... | collective-permute-start | bytes 393224 | tf_op jit(solution)/shard_map/ppermute | solution.py:28
  32.4 12.9 %collective-permute-start.12 = (bf16[128,512]{1,0:T(8,128)(2,1)S(1)}, bf16[128,512]{1,0:T(8,128)(2,1)S(1)}, u32[]{:S(2)}, u32[]{:S(2)}) collective-permute-start(bf16[128,512]{1,0:T(8,128)(2,1)S(1)} %dynamic-slice_bitcast_fusion), channel_id=1, source_target_pairs={{0,4},{4,0},{8,12},{12,8},{1,5},{5,1},{9,13},{13,9},{2,6},{6,2},{1... | collective-permute-start | bytes 393224 | tf_op jit(solution)/shard_map/ppermute | solution.py:28
  37.6 1.3 %collective-permute-start.9 = (f32[16,640]{1,0:T(8,128)S(1)}, f32[16,640]{1,0:T(8,128)S(1)}, u32[]{:S(2)}, u32[]{:S(2)}) collective-permute-start(f32[16,640]{1,0:T(8,128)S(1)} %get-tuple-element.49), channel_id=1, source_target_pairs={{0,1},{1,0},{2,3},{3,2},{4,5},{5,4},{6,7},{7,6},{8,9},{9,8},{10,11... | collective-permute-start | bytes 122888 | tf_op jit(solution)/shard_map/ppermute | solution.py:28
  37.7 4.1 %collective-permute-start.10 = (f32[16,640]{1,0:T(8,128)S(1)}, f32[16,640]{1,0:T(8,128)S(1)}, u32[]{:S(2)}, u32[]{:S(2)}) collective-permute-start(f32[16,640]{1,0:T(8,128)S(1)} %get-tuple-element.50), channel_id=1, source_target_pairs={{0,2},{1,3},{2,0},{3,1},{4,6},{5,7},{6,4},{7,5},{8,10},{9,11},{10,... | collective-permute-start | bytes 122888 | tf_op jit(solution)/shard_map/ppermute | solution.py:28
  38.9 3.5 %collective-permute-start.11 = (f32[16,640]{1,0:T(8,128)S(1)}, f32[16,640]{1,0:T(8,128)S(1)}, u32[]{:S(2)}, u32[]{:S(2)}) collective-permute-start(f32[16,640]{1,0:T(8,128)S(1)} %get-tuple-element.51), channel_id=1, source_target_pairs={{0,3},{1,2},{2,1},{3,0},{4,7},{5,6},{6,5},{7,4},{8,11},{9,10},{10,... | collective-permute-start | bytes 122888 | tf_op jit(solution)/shard_map/ppermute | solution.py:28
  45.3 12.7 %collective-permute-start.13 = (bf16[128,512]{1,0:T(8,128)(2,1)S(1)}, bf16[128,512]{1,0:T(8,128)(2,1)S(1)}, u32[]{:S(2)}, u32[]{:S(2)}) collective-permute-start(bf16[128,512]{1,0:T(8,128)(2,1)S(1)} %collective-permute-done.12.rest_0_), channel_id=1, source_target_pairs={{0,16},{16,0},{1,17},{17,1},{2,18},{18,2},{3,19},{19,3},{4,20},{20... | collective-permute-start | bytes 393224 | tf_op jit(solution)/shard_map/ppermute | solution.py:28
  45.9 12.1 %collective-permute-start.15 = (bf16[128,512]{1,0:T(8,128)(2,1)S(1)}, bf16[128,512]{1,0:T(8,128)(2,1)S(1)}, u32[]{:S(2)}, u32[]{:S(2)}) collective-permute-start(bf16[128,512]{1,0:T(8,128)(2,1)S(1)} %collective-permute-done.14.rest_2_), channel_id=1, source_target_pairs={{0,16},{16,0},{1,17},{17,1},{2,18},{18,2},{3,19},{19,3},{4,20},{20... | collective-permute-start | bytes 393224 | tf_op jit(solution)/shard_map/ppermute | solution.py:28
  47.4 10.6 %collective-permute-start.17 = (bf16[128,512]{1,0:T(8,128)(2,1)S(1)}, bf16[128,512]{1,0:T(8,128)(2,1)S(1)}, u32[]{:S(2)}, u32[]{:S(2)}) collective-permute-start(bf16[128,512]{1,0:T(8,128)(2,1)S(1)} %collective-permute-done.16.rest_4_), channel_id=1, source_target_pairs={{0,16},{16,0},{1,17},{17,1},{2,18},{18,2},{3,19},{19,3},{4,20},{20... | collective-permute-start | bytes 393224 | tf_op jit(solution)/shard_map/ppermute | solution.py:28
  48.0 10.1 %all-to-all-start.1 = ((bf16[16,16,128]{2,1,0:T(8,128)(2,1)}), bf16[16,16,128]{2,1,0:T(8,128)(2,1)S(1)}, u32[]{:S(2)}, u32[]{:S(2)}) async-start(bf16[16,16,128]{2,1,0:T(8,128)(2,1)} %get-tuple-element.52), calls=%async_computation.1 | async-start | bytes 131072 | tf_op jit(solution)/shard_map/all_to_all | solution.py:286
